TPU v7x, 32 devices: a whole 2x2x4 slice. The times are simulated.
32 devices in a mesh: sp: 8 (over z, y), tp: 4 (over x, core).
Axes of the slice: x: 2, y: 2, z: 4, core: 2. Of those that a mesh axis runs over, the one named last changes fastest.
Arguments:
- stream: bfloat16 [4096, 2048], P(('sp', 'tp')), may hold values from -6 to 6
- query_rows: bfloat16 [4096, 1024], P('sp', 'tp'), may hold values from -6 to 6
- key_rows: bfloat16 [4096, 1024], P('sp', 'tp'), may hold values from -6 to 6
- value_rows: bfloat16 [4096, 1024], P('sp', 'tp'), may hold values from -6 to 6
- log_decay: float32 [4096, 1024], P('sp', 'tp'), may hold values from -0.8 to 0, as said below
- head_gain: float32 [1024], P('tp'), may hold values from 0.1 to 1.9
- out_weight: bfloat16 [1024, 2048], replicated, may hold values from -0.1875 to 0.1875
- ffn_gain: float32 [2048], replicated, may hold values from 0.1 to 1.9
- expert_ids: int32 [4096, 2], P(('sp', 'tp')), may hold values from 0 to 31, as said below
- group_prob: float32 [4096], P(('sp', 'tp')), may hold values from 0.3 to 1
- pick_logits: float32 [4096, 2], P(('sp', 'tp')), may hold values from -6 to 6
- gate_weight: bfloat16 [32, 2048, 1024], P(('sp', 'tp')), may hold values from -0.125 to 0.125
- up_weight: bfloat16 [32, 2048, 1024], P(('sp', 'tp')), may hold values from -0.125 to 0.125
- down_weight: bfloat16 [32, 1024, 2048], P(('sp', 'tp')), may hold values from -0.1875 to 0.1875
Outputs:
- layer_out: bfloat16 [4096, 2048], P(('sp', 'tp'))
Inputs may be any that keep to these rules, and one draw needn't show every extreme that they name: `log_decay`: entries are negative. `expert_ids`: A token's two experts are different and lie in one group of 8 consecutive expert numbers. Among the 128 tokens of one device (aligned blocks of 128 tokens) no expert is named more than 16 times; in every draw the experts of one group are each named exactly 16 times by the tokens of every device.
All inputs are finite; a program needn't handle non-finite values.
Results may differ from a plain program's by a relative error of at most 0.014.
Values may be sent and summed in bfloat16 or wider, within the bound.
A program may use at most 128 MiB of HBM per device.

v0:
```python
import jax
import jax.numpy as jnp
from jax import lax
from jax.sharding import PartitionSpec as P

KEY_FEATURE_DIM = 128
TOPK = 2
BLOCK = 64
EXP_DEV = 1


PRECISE = lax.Precision.HIGHEST
EPSILON = 1e-06


def entering_2(value, axis, combine, identity):
    devices, mine = (lax.axis_size(axis), lax.axis_index(axis))
    everything = jax.tree.map(lambda part: lax.all_gather(part, axis), value)
    start = jax.tree.map(
        lambda part, zero: jnp.broadcast_to(jnp.asarray(zero, part.dtype), part.shape),
        value,
        identity,
    )

    def turn(k, before):
        reached = k < mine
        new = combine(before, jax.tree.map(lambda part: part[k], everything))
        return jax.tree.map(lambda a, b: jnp.where(reached, a, b), new, before)

    return lax.fori_loop(0, devices, turn, start)


def gla_local(query_rows, key_rows, value_rows, log_decay):
    token_count, col_count = query_rows.shape
    head_count = col_count // KEY_FEATURE_DIM
    blocks = token_count // BLOCK
    block_shape = (blocks, BLOCK, head_count, KEY_FEATURE_DIM)
    query_all = query_rows.astype(jnp.float32).reshape(block_shape) * KEY_FEATURE_DIM ** (-0.5)
    key_all = key_rows.astype(jnp.float32).reshape(block_shape)
    value_all = value_rows.astype(jnp.float32).reshape(block_shape)
    cumulative = jnp.cumsum(log_decay.reshape(block_shape), axis=1)
    q_dec = query_all * jnp.exp(cumulative)
    k_dec = key_all * jnp.exp(-cumulative)
    scores = jnp.einsum("nihd,njhd->nhij", q_dec, k_dec, precision=PRECISE)
    positions = jnp.arange(BLOCK, dtype=jnp.int32)
    causal = positions[:, None] >= positions[None, :]
    scores = jnp.where(causal[None, None], scores, jnp.float32(0.0))
    in_block = jnp.einsum("nhij,njhe->nihe", scores, value_all, precision=PRECISE)
    block_fall = cumulative[:, -1]
    key_last = key_all * jnp.exp(block_fall[:, None] - cumulative)
    update = jnp.einsum("njhd,njhe->nhde", key_last, value_all, precision=PRECISE)

    def advance(carry_state, step_input):
        block_update, fall_here = step_input
        return (carry_state * jnp.exp(fall_here)[:, :, None] + block_update, carry_state)

    local_state, entering = lax.scan(
        advance,
        jnp.zeros((head_count, KEY_FEATURE_DIM, KEY_FEATURE_DIM), jnp.float32),
        (update, block_fall),
    )
    within = in_block + jnp.einsum("nihd,nhde->nihe", q_dec, entering, precision=PRECISE)
    block_start = jnp.cumsum(block_fall, axis=0) - block_fall
    read_weight = query_all * jnp.exp(cumulative + block_start[:, None])
    fall_all = jnp.exp(jnp.sum(block_fall, axis=0))
    return (within, read_weight, local_state, fall_all)


def compose(earlier, later):
    return (earlier[0] * later[1][:, :, None] + later[0], earlier[1] * later[1])


def run_experts(arrived, gate_weight, up_weight, down_weight):
    gate_act = jnp.einsum(
        "sekd,edf->sekf", arrived, gate_weight, preferred_element_type=jnp.float32
    )
    up_act = jnp.einsum("sekd,edf->sekf", arrived, up_weight, preferred_element_type=jnp.float32)
    hidden = (jax.nn.silu(gate_act) * up_act).astype(jnp.bfloat16)
    return jnp.einsum(
        "sekf,efd->sekd", hidden, down_weight, preferred_element_type=jnp.float32
    ).astype(jnp.bfloat16)


def local(
    stream,
    query_rows,
    key_rows,
    value_rows,
    log_decay,
    head_gain,
    out_weight,
    ffn_gain,
    expert_ids,
    group_prob,
    pick_logits,
    gate_weight,
    up_weight,
    down_weight,
):
    within, read_weight, local_state, fall_all = gla_local(
        query_rows, key_rows, value_rows, log_decay
    )
    identity = (jnp.zeros_like(local_state), jnp.ones_like(fall_all))
    incoming, _ = entering_2((local_state, fall_all), "sp", compose, identity)
    heads_out = within + jnp.einsum("nihd,hde->nihe", read_weight, incoming, precision=PRECISE)
    token_count, head_cols = query_rows.shape
    head_count = head_cols // KEY_FEATURE_DIM
    heads_out = heads_out.reshape(token_count, head_count, KEY_FEATURE_DIM)
    mean_sq = jnp.mean(heads_out * heads_out, axis=-1, keepdims=True)
    attn_rows = (
        heads_out * lax.rsqrt(mean_sq + EPSILON) * head_gain.reshape(head_count, KEY_FEATURE_DIM)
    )
    attn_rows = attn_rows.reshape(token_count, head_cols).astype(jnp.bfloat16)
    tp_size = lax.axis_size("tp")
    sp_size = lax.axis_size("sp")
    row_count = token_count // tp_size
    projected = jnp.dot(
        lax.all_to_all(
            attn_rows.reshape(tp_size, row_count, head_cols),
            "tp",
            split_axis=0,
            concat_axis=2,
            tiled=True,
        )[0],
        out_weight,
        preferred_element_type=jnp.float32,
    )[None][0]
    mixed32 = (stream.astype(jnp.float32) + projected).astype(jnp.bfloat16).astype(jnp.float32)
    normed = (
        mixed32
        * lax.rsqrt(jnp.mean(mixed32 * mixed32, axis=-1, keepdims=True) + EPSILON)
        * ffn_gain
    )
    normed = normed.astype(jnp.bfloat16)
    model_width = normed.shape[1]
    devices = sp_size * tp_size
    experts_all = EXP_DEV * devices
    slot_cap = 2 * row_count * TOPK // experts_all
    flat_ids = expert_ids.reshape(-1)
    onehot = (flat_ids[:, None] == jnp.arange(experts_all, dtype=jnp.int32)[None, :]).astype(
        jnp.int32
    )
    slot_rank = jnp.sum(jnp.cumsum(onehot, axis=0) * onehot, axis=1) - 1
    slot_dest = flat_ids * slot_cap + slot_rank
    token_index = jnp.arange(row_count * TOPK, dtype=jnp.int32) // TOPK
    source = (
        jnp.full((experts_all * slot_cap,), row_count, jnp.int32).at[slot_dest].set(token_index)
    )
    padded = jnp.concatenate([normed, jnp.zeros((1, model_width), jnp.bfloat16)], axis=0)
    outgoing = padded[source]
    served = run_experts(
        lax.all_to_all(
            outgoing.reshape(devices, EXP_DEV, slot_cap, model_width),
            ("sp", "tp"),
            split_axis=0,
            concat_axis=0,
            tiled=True,
        ),
        gate_weight,
        up_weight,
        down_weight,
    )
    returned = lax.all_to_all(served, ("sp", "tp"), split_axis=0, concat_axis=0, tiled=True)
    back_rows = returned.reshape(experts_all * slot_cap, model_width)
    picked = back_rows[slot_dest].reshape(row_count, TOPK, model_width)
    logit_gap = pick_logits[:, 0] - pick_logits[:, 1]
    first_weight = group_prob * jax.nn.sigmoid(logit_gap)
    second_weight = group_prob * jax.nn.sigmoid(-logit_gap)
    branch = first_weight[:, None] * picked[:, 0].astype(jnp.float32) + second_weight[
        :, None
    ] * picked[:, 1].astype(jnp.float32)
    return (mixed32 + branch).astype(jnp.bfloat16)


def solution(mesh):
    in_specs = (
        P(("sp", "tp"), None),
        P("sp", "tp"),
        P("sp", "tp"),
        P("sp", "tp"),
        P("sp", "tp"),
        P("tp"),
        P(),
        P(),
        P(("sp", "tp"), None),
        P(("sp", "tp")),
        P(("sp", "tp"), None),
        P(("sp", "tp"), None, None),
        P(("sp", "tp"), None, None),
        P(("sp", "tp"), None, None),
    )
    out_specs = P(("sp", "tp"), None)
    return jax.shard_map(local, mesh=mesh, in_specs=in_specs, out_specs=out_specs, check_vma=False)
```

profile of v0, /device:TPU:0, one launch (start us, length us, event | category | flops | bytes accessed | tf_op | source)
XLA Modules:
  0.0 223.7 jit_solution(18401733635667023572)
XLA Ops:
  6.5 1.4 reshape.185
  7.9 0.4 fusion.43
  8.3 0.6 slice_bitcast_fusion
  9.0 0.3 mul.148
  9.3 0.3 reshape.200
  9.6 0.7 exponential_multiply_fusion.3
  10.4 1.0 fusion.40
  11.4 6.6 %while.27 = (s32[]{:T(128)}, f32[2,128,128]{2,1,0:T(8,128)S(1)}, f32[8,2,128,128]{3,2,1,0:T(8,128)}, f32[8,2,128]{2,0,1:T(8,128)S(1)}, f32[8,2,128,128]{3,2,1,0:T(8,128)S(1)}, /*index=5*/s32[]{:T(128)}, s32[]{:T(128)}) while((s32[]{:T(128)}, f32[2,128,128]{2,1,0:T(8,128)S(1)}, f32[8,2,128,128]{3,2,1,0:T(8,128)}, ...), condition=%wide.region_2.3_spmd.clone, body=%wide.region_1.2_spmd.clone.sunk | while | flops 131075 | bytes 661088 | solution.py:57
  11.4 0.7 bitcast_dynamic-update-slice_fusion.2
  12.1 0.1 bitcast_add_fusion.3
  12.2 0.7 bitcast_dynamic-update-slice_fusion.2
  12.9 0.1 bitcast_add_fusion.3
  13.1 0.7 bitcast_dynamic-update-slice_fusion.2
  13.7 0.1 bitcast_add_fusion.3
  13.9 0.7 bitcast_dynamic-update-slice_fusion.2
  14.6 0.1 bitcast_add_fusion.3
  14.7 0.7 bitcast_dynamic-update-slice_fusion.2
  15.5 0.7 bitcast_dynamic-update-slice_fusion.2
  16.2 0.1 bitcast_add_fusion.3
  16.4 0.7 bitcast_dynamic-update-slice_fusion.2
  17.2 0.7 bitcast_dynamic-update-slice_fusion.2
  18.0 0.6 copy-done
  18.8 0.1 eq.29
  19.0 0.1 eq.25
  19.1 0.6 reduce-window.6
  19.7 0.2 slice_reduce_fusion
  20.1 0.1 mul.168
  20.3 1.4 scatter_custom_fusion
  21.8 22.3 %all-gather.2 = f32[8,2,128]{2,1,0:T(2,128)S(1)} all-gather(f32[1,2,128]{2,1,0:T(2,128)S(1)} %exponential_bitcast_fusion.1), channel_id=2, replica_groups=mesh['sp'=8,'tp'=4] {'sp'}, dimensions={0}, use_global_device_ids=true | all-gather | bytes 9216 | tf_op jit(solution)/shard_map/all_gather | solution.py:18
  44.1 1.1 convolution_select_fusion
  45.2 0.4 convolution_bitcast_fusion.2
  45.6 16.3 %all-gather.5.cloned.1.call-done = f32[16,128,128]{2,1,0:T(8,128)} async-done(((f32[2,128,128]{2,1,0:T(8,128)}), f32[16,128,128]{2,1,0:T(8,128)}) %all-gather.5.cloned.1.call-update) | async-done | bytes 1048592 | tf_op jit(solution)/shard_map/all_gather | solution.py:18
  61.9 8.6 %while.28 = (s32[]{:T(128)}, f32[2,128,128]{2,1,0:T(8,128)S(1)}, s32[]{:T(128)}, f32[8,2,128]{2,1,0:T(2,128)S(1)}, f32[8,2,128,128]{3,2,1,0:T(8,128)}, /*index=5*/s32[]{:T(128)}, s32[]{:T(128)}) while((s32[]{:T(128)}, f32[2,128,128]{2,1,0:T(8,128)S(1)}, s32[]{:T(128)}, f32[8,2,128]{2,1,0:T(2,128)S(1)}, ...), condition=%wide.region_5.6_spmd.clone, body=%wide.region_4.5_spmd.clone.sunk | while | flops 131076 | bytes 396393 | solution.py:30
  61.9 1.0 fusion.64
  63.0 1.0 fusion.64
  64.0 1.0 fusion.64
  65.1 1.0 fusion.64
  66.2 1.0 fusion.64
  67.3 1.0 fusion.64
  68.4 1.0 fusion.64
  69.4 1.0 fusion.64
  70.5 0.6 convolution_bitcast_fusion
  71.1 1.2 multiply_reduce_fusion.1
  72.3 0.1 copy.116
  72.5 0.6 mul.154
  73.1 0.4 mul.155
  73.5 0.4 copy.104
  73.9 0.4 reshape.189
  74.4 0.8 multiply_convert_fusion.1
  75.2 3.6 %all-to-all-start = ((bf16[4,128,256]{2,1,0:T(8,128)(2,1)}), bf16[4,128,256]{2,1,0:T(8,128)(2,1)S(1)}, u32[]{:S(2)}, u32[]{:S(2)}) async-start(bf16[4,128,256]{2,1,0:T(8,128)(2,1)} %multiply_convert_fusion.1), calls=%async_computation | async-start | bytes 524288 | tf_op jit(solution)/shard_map/all_to_all | solution.py:118
  78.8 5.8 %all-to-all-done = bf16[4,128,256]{2,1,0:T(8,128)(2,1)S(1)} async-done(((bf16[4,128,256]{2,1,0:T(8,128)(2,1)}), bf16[4,128,256]{2,1,0:T(8,128)(2,1)S(1)}, u32[]{:S(2)}, u32[]{:S(2)}) %all-to-all-start) | async-done | bytes 262176 | tf_op jit(solution)/shard_map/all_to_all | solution.py:118
  84.5 0.2 copy.107
  84.7 3.0 %multiply_reduce_fusion = (f32[128]{0:T(128)S(1)}, f32[128,2048]{1,0:T(8,128)S(1)}) fusion(bf16[128,1024]{0,1:T(8,128)(2,1)S(1)} %bitcast.169, bf16[1024,2048]{1,0:T(8,128)(2,1)} %param.24, bf16[128,2048]{1,0:T(8,128)(2,1)S(1)} %copy-done.2), kind=kOutput, calls=%fused_computation.43 | convolution fusion | flops 538443648 | bytes 6029824 | tf_op jit(solution)/shard_map/dot_general | solution.py:117
  87.8 0.2 multiply_convert_fusion
  88.0 3.3 %gather_fusion = bf16[512,2048]{1,0:T(8,128)(2,1)} fusion(bf16[129,2048]{1,0:T(8,128)(2,1)S(1)} %concatenate.3, s32[1024]{0:T(1024)S(1)} %pad_clamp_fusion.1), kind=kCustom, calls=%fused_computation | custom fusion | bytes 4196352 | tf_op jit(solution)/shard_map/gather | solution.py:150
  91.3 51.9 %all_to_all.25 = bf16[32,1,16,2048]{3,2,1,0:T(8,128)(2,1)S(1)} all-to-all(bf16[32,1,16,2048]{3,2,1,0:T(8,128)(2,1)} %bitcast.168), channel_id=1, replica_groups=mesh['sp'=8,'tp'=4] {'sp','tp'}, dimensions={0} | all-to-all | bytes 4194304 | tf_op jit(solution)/shard_map/all_to_all | solution.py:152
  143.2 3.7 %fusion.3 = f32[32,16,1024]{2,1,0:T(8,128)} fusion(bf16[1,2048,1024]{2,1,0:T(8,128)(2,1)S(1)} %copy-done.12, bf16[32,1,16,2048]{3,2,1,0:T(8,128)(2,1)S(1)} %all_to_all.25), kind=kOutput, calls=%fused_computation.12 | convolution fusion | flops 2147483648 | bytes 8388608 | tf_op jit(solution)/shard_map/sekd,edf->sekf/dot_general | solution.py:77
  146.9 10.0 %fusion.10 = bf16[32,1,16,2048]{3,2,1,0:T(8,128)(2,1)} fusion(bf16[1,1024,2048]{2,1,0:T(8,128)(2,1)} %param.31, f32[32,16,1024]{2,1,0:T(8,128)} %fusion.3, bf16[1,2048,1024]{2,1,0:T(8,128)(2,1)} %param.29, bf16[32,1,16,2048]{3,2,1,0:T(8,128)(2,1)S(1)} %all_to_all.25), kind=kOutput, calls=%fused_computation.17 | convolution fusion | flops 4299161600 | bytes 14680064 | tf_op jit(solution)/shard_map/sekf,efd->sekd/dot_general | solution.py:79
  157.0 3.6 %all-to-all-start.2 = ((bf16[32,1,16,2048]{3,2,1,0:T(8,128)(2,1)}), bf16[32,1,16,2048]{3,2,1,0:T(8,128)(2,1)S(1)}, u32[]{:S(2)}, u32[]{:S(2)}) async-start(bf16[32,1,16,2048]{3,2,1,0:T(8,128)(2,1)} %fusion.10), calls=%async_computation.2 | async-start | bytes 4194304 | tf_op jit(solution)/shard_map/all_to_all | solution.py:163
  160.6 48.7 %all-to-all-done.2 = bf16[32,1,16,2048]{3,2,1,0:T(8,128)(2,1)S(1)} async-done(((bf16[32,1,16,2048]{3,2,1,0:T(8,128)(2,1)}), bf16[32,1,16,2048]{3,2,1,0:T(8,128)(2,1)S(1)}, u32[]{:S(2)}, u32[]{:S(2)}) %all-to-all-start.2) | async-done | bytes 2097184 | tf_op jit(solution)/shard_map/all_to_all | solution.py:163
  209.3 2.3 %gather_fusion.1 = bf16[256,2048]{1,0:T(8,128)(2,1)} fusion(bf16[512,2048]{1,0:T(8,128)(2,1)S(1)} %bitcast.167, s32[1024]{0:T(1024)S(1)} %pad_clamp_fusion), kind=kCustom, calls=%fused_computation.1 | custom fusion | bytes 2098176 | tf_op jit(solution)/shard_map/gather | solution.py:165
  211.7 1.7 reshape.198
  213.4 1.5 fusion.58
  214.9 1.9 fusion.34
  (80 shorter events, 1.2 us)
Async XLA Ops:
  6.5 2.4 %copy-start.3 = (bf16[512,256]{1,0:T(8,128)(2,1)S(1)}, bf16[512,256]{1,0:T(8,128)(2,1)}, u32[]{:S(2)}) copy-start(bf16[512,256]{1,0:T(8,128)(2,1)} %param.19) | copy-start | bytes 786436
  6.5 2.7 %copy-start.4 = (bf16[512,256]{1,0:T(8,128)(2,1)S(1)}, bf16[512,256]{1,0:T(8,128)(2,1)}, u32[]{:S(2)}) copy-start(bf16[512,256]{1,0:T(8,128)(2,1)} %param.20) | copy-start | bytes 786436
  6.5 55.3 %all-gather.5.cloned.1.call-start = ((), (), s32[]{:S(2)}) async-start(), calls=%async_computation.3 | async-start | bytes 1179648 | tf_op jit(solution)/shard_map/all_gather | solution.py:18
  7.9 1.6 copy-start.5
  11.4 7.3 %copy-start.7 = (s32[128,2]{0,1:T(2,128)S(1)}, s32[128,2]{0,1:T(2,128)}, u32[]{:S(2)}) copy-start(s32[128,2]{0,1:T(2,128)} %param.26) | copy-start | bytes 3076
  11.4 10.4 %copy-start.8 = (f32[2,128]{1,0:T(2,128)S(1)}, f32[2,128]{1,0:T(2,128)}, u32[]{:S(2)}) copy-start(f32[2,128]{1,0:T(2,128)} %get-tuple-element.220) | copy-start | bytes 3076
  18.0 0.7 copy-start
  45.2 26.0 %copy-start.1 = (f32[8,2,128,128]{3,2,1,0:T(8,128)S(1)}, f32[8,2,128,128]{3,2,1,0:T(8,128)}, u32[]{:S(2)}) copy-start(f32[8,2,128,128]{3,2,1,0:T(8,128)} %get-tuple-element.127) | copy-start | bytes 3145732
  72.3 2.1 copy-start.10
  73.5 11.2 %copy-start.2 = (bf16[128,2048]{1,0:T(8,128)(2,1)S(1)}, bf16[128,2048]{1,0:T(8,128)(2,1)}, u32[]{:S(2)}) copy-start(bf16[128,2048]{1,0:T(8,128)(2,1)} %param.18) | copy-start | bytes 1572868
  75.2 9.4 %all-to-all-start = ((bf16[4,128,256]{2,1,0:T(8,128)(2,1)}), bf16[4,128,256]{2,1,0:T(8,128)(2,1)S(1)}, u32[]{:S(2)}, u32[]{:S(2)}) async-start(bf16[4,128,256]{2,1,0:T(8,128)(2,1)} %multiply_convert_fusion.1), calls=%async_computation | async-start | bytes 524288 | tf_op jit(solution)/shard_map/all_to_all | solution.py:118
  84.7 3.0 %copy-start.6 = (f32[2048]{0:T(1024)S(1)}, f32[2048]{0:T(1024)}, u32[]{:S(2)}) copy-start(f32[2048]{0:T(1024)} %param.25) | copy-start | bytes 24580
  91.3 51.9 %copy-start.12 = (bf16[1,2048,1024]{2,1,0:T(8,128)(2,1)S(1)}, bf16[1,2048,1024]{2,1,0:T(8,128)(2,1)}, u32[]{:S(2)}) copy-start(bf16[1,2048,1024]{2,1,0:T(8,128)(2,1)} %param.30) | copy-start | bytes 12582916
  157.0 3.6 %copy-start.9 = (f32[128,2]{0,1:T(2,128)S(1)}, f32[128,2]{0,1:T(2,128)}, u32[]{:S(2)}) copy-start(f32[128,2]{0,1:T(2,128)} %param.28) | copy-start | bytes 3076
  157.0 3.6 %copy-start.11 = (f32[128]{0:T(128)S(1)}, f32[128]{0:T(128)}, u32[]{:S(2)}) copy-start(f32[128]{0:T(128)} %param.27) | copy-start | bytes 1540
  157.0 52.3 %all-to-all-start.2 = ((bf16[32,1,16,2048]{3,2,1,0:T(8,128)(2,1)}), bf16[32,1,16,2048]{3,2,1,0:T(8,128)(2,1)S(1)}, u32[]{:S(2)}, u32[]{:S(2)}) async-start(bf16[32,1,16,2048]{3,2,1,0:T(8,128)(2,1)} %fusion.10), calls=%async_computation.2 | async-start | bytes 4194304 | tf_op jit(solution)/shard_map/all_to_all | solution.py:163
Sparse Core Ops, SparseCore 0:
  18.8 43.0 all-gather.4
where the time goes:
time: 224 us
  blocking collectives  74.2 us (33%)
  waiting for transfers between devices  70.8 us (32%)
  matrix products  21 us (9%)
  other arithmetic  20 us (9%)
  local copies, waits for them, and re-layouts  16.2 us (7%)
  between operations  13.8 us (6%)
  starting transfers between devices  7.18 us (3%)
    all_to_all x1, blocking collectives, local(): lax.all_to_all(outgoing.reshape(devices, EXP_DEV, slot_cap, model_width),...  51.9 us
    all_to_all x1, waiting for transfers between devices, local(): lax.all_to_all(served, ('sp', 'tp'), split_axis=0, concat_axis=0, tiled=T...  48.7 us
    all_gather x1, blocking collectives, entering_2(): everything = jax.tree.map(lambda part: lax.all_gather(part, axis), value)  22.3 us
    all_gather x1, waiting for transfers between devices, entering_2(): everything = jax.tree.map(lambda part: lax.all_gather(part, axis), value)  16.3 us
    dot_general x1, matrix products, run_experts(): jnp.einsum('sekf,efd->sekd', hidden, down_weight, preferred_element_type=...  10 us
    select_n x8, other arithmetic, turn(): return jax.tree.map(lambda a, b: jnp.where(reached, a, b), new, before)  8.28 us
    all_to_all x1, waiting for transfers between devices, local(): lax.all_to_all(attn_rows.reshape(tp_size, row_count, head_cols), 'tp', sp...  5.77 us
    dynamic_update_slice x8, other arithmetic, gla_local(): lax.scan(advance, jnp.zeros((head_count, KEY_FEATURE_DIM, KEY_FEATURE_DIM...  5.29 us
  transfers between devices with their start and end apart: 3, of which 3 were waited for; matrix products, arithmetic and copies ran while one was open for 2% of the time, Pallas kernels for 0%

commit v1 on v0

v1 whole, which is shorter than its diff:
```python
import functools

import jax
import jax.numpy as jnp
from jax import lax
from jax.experimental import pallas as pl
from jax.experimental.pallas import tpu as pltpu
from jax.sharding import PartitionSpec as P

KEY_FEATURE_DIM = 128
TOPK = 2
BLOCK = 64
GROUPS = 4
EPSILON = 1e-06
F32 = jnp.float32
BF16 = jnp.bfloat16
MESH = pl.DeviceIdType.MESH
VMEM_LIMIT = 60 * 1024 * 1024


def dot(a, b):
    return jnp.dot(a, b, preferred_element_type=F32)


def dot_nt(a, b):
    return lax.dot_general(a, b, (((1,), (1,)), ((), ())), preferred_element_type=F32)


def dot_tn(a, b):
    return lax.dot_general(a, b, (((0,), (0,)), ((), ())), preferred_element_type=F32)


def iota(shape, axis):
    return lax.broadcasted_iota(jnp.int32, shape, axis)


def mixer_kernel(
    n_sp, n_tp, capp,
    q_ref, k_ref, v_ref, decay_ref, gain_ref, stream_ref, ow_hbm, ffn_ref, ids_ref, prob_ref,
    logit_ref,
    mixed_ref, rows_ref, wc_ref, gsel_ref,
    qd, kd, rw, st_in, within, ow, inc_s, inc_f, exc_s, exc_f,
    s_send, s_recv, f_send, f_recv, attn, arecv,
    ow_sem, ss_sem, sr_sem, fs_sem, fr_sem, as_sem, ar_sem,
):
    me, tp = lax.axis_index("sp"), lax.axis_index("tp")
    tokens, cols = q_ref.shape
    heads = cols // KEY_FEATURE_DIM
    blocks = tokens // BLOCK
    row_count = stream_ref.shape[0]
    model = stream_ref.shape[1]
    steps = s_send.shape[0]

    barrier = pltpu.get_barrier_semaphore()
    for i in range(1, n_sp):
        pl.semaphore_signal(
            barrier, inc=1, device_id=(lax.rem(me + i, n_sp), tp), device_id_type=MESH)
    for i in range(1, n_tp):
        pl.semaphore_signal(
            barrier, inc=1, device_id=(me, lax.rem(tp + i, n_tp)), device_id_type=MESH)
    ow_copy = pltpu.make_async_copy(ow_hbm, ow, ow_sem)
    ow_copy.start()

    tri = (iota((BLOCK, BLOCK), 0) >= iota((BLOCK, BLOCK), 1)).astype(F32)
    tri16 = tri.astype(BF16)
    scale = KEY_FEATURE_DIM ** (-0.5)
    state = [jnp.zeros((KEY_FEATURE_DIM, KEY_FEATURE_DIM), F32) for _ in range(heads)]
    start = jnp.zeros((1, cols), F32)
    for n in range(blocks):
        rows = slice(n * BLOCK, (n + 1) * BLOCK)
        g = decay_ref[rows, :]
        hi = g.astype(BF16)
        rest = g - hi.astype(F32)
        mid = rest.astype(BF16)
        low = (rest - mid.astype(F32)).astype(BF16)
        cum = dot(tri16, hi) + dot(tri16, mid) + dot(tri16, low)
        fall = cum[BLOCK - 1 : BLOCK, :]
        kf = k_ref[rows, :].astype(F32)
        q_dec = q_ref[rows, :].astype(F32) * scale * jnp.exp(cum)
        qd[rows, :] = q_dec.astype(BF16)
        rw[rows, :] = (q_dec * jnp.exp(start)).astype(BF16)
        kd[rows, :] = (kf * jnp.exp(-cum)).astype(BF16)
        k_last = (kf * jnp.exp(fall - cum)).astype(BF16)
        keep = jnp.exp(fall)
        for h in range(heads):
            ch = slice(h * KEY_FEATURE_DIM, (h + 1) * KEY_FEATURE_DIM)
            st_in[n, h] = state[h].astype(BF16)
            state[h] = state[h] * keep[:, ch] + dot_tn(v_ref[rows, ch], k_last[:, ch])
        start = start + fall
    for h in range(heads):
        inc_s[h] = state[h]
        exc_s[h] = jnp.zeros_like(state[h])
    inc_f[...] = jnp.broadcast_to(jnp.exp(start), inc_f.shape)
    exc_f[...] = jnp.ones_like(exc_f)

    pl.semaphore_wait(barrier, n_sp - 1 + n_tp - 1)

    def state_copies(s):
        to = (lax.rem(me + 2 ** s, n_sp), tp)
        return (
            pltpu.make_async_remote_copy(
                s_send.at[s], s_recv.at[s], ss_sem.at[s], sr_sem.at[s],
                device_id=to, device_id_type=MESH),
            pltpu.make_async_remote_copy(
                f_send.at[s], f_recv.at[s], fs_sem.at[s], fr_sem.at[s],
                device_id=to, device_id_type=MESH),
        )

    def send_state(s):
        s_send[s] = inc_s[...].astype(BF16)
        f_send[s] = inc_f[...]

        @pl.when(me + 2 ** s < n_sp)
        def _():
            for copy in state_copies(s):
                copy.start()

    send_state(0)

    experts = n_sp * n_tp
    per_group = experts // GROUPS
    group_cap = rows_ref.shape[0] // GROUPS
    slots = per_group * capp
    ids = ids_ref[...]
    id0, id1 = ids[:, 0:1], ids[:, 1:2]
    oh0 = (iota((row_count, experts), 1) == id0).astype(F32)
    oh1 = (iota((row_count, experts), 1) == id1).astype(F32)
    before = (iota((row_count, row_count), 0) > iota((row_count, row_count), 1)).astype(BF16)
    counts = dot(before, (oh0 + oh1).astype(BF16))
    rank0 = jnp.sum(counts * oh0, axis=1, keepdims=True).astype(jnp.int32)
    rank1 = jnp.sum(counts * oh1, axis=1, keepdims=True).astype(jnp.int32)
    group = id0 // per_group
    ohg = (iota((row_count, KEY_FEATURE_DIM), 1) == group).astype(F32)
    rank_g = jnp.sum(dot(before, ohg.astype(BF16)) * ohg, axis=1, keepdims=True).astype(jnp.int32)
    place = group * group_cap + rank_g
    gsel = (iota((row_count, GROUPS * group_cap), 1) == place).astype(F32).astype(BF16)
    gsel_ref[...] = gsel
    slot0 = (id0 - group * per_group) * capp + rank0
    slot1 = (id1 - group * per_group) * capp + rank1
    logits = logit_ref[...]
    gap = logits[:, 0:1] - logits[:, 1:2]
    w0 = prob_ref[...] / (1.0 + jnp.exp(-gap))
    w1 = prob_ref[...] / (1.0 + jnp.exp(gap))
    slot_iota = iota((row_count, slots), 1)
    w_tok = jnp.where(slot_iota == slot0, w0, 0.0) + jnp.where(slot_iota == slot1, w1, 0.0)
    wc_ref[...] = dot_tn(gsel, w_tok.astype(BF16)).astype(BF16)

    for n in range(blocks):
        rows = slice(n * BLOCK, (n + 1) * BLOCK)
        for h in range(heads):
            ch = slice(h * KEY_FEATURE_DIM, (h + 1) * KEY_FEATURE_DIM)
            scores = jnp.where(tri > 0, dot_nt(qd[rows, ch], kd[rows, ch]), 0.0)
            within[rows, ch] = dot(scores.astype(BF16), v_ref[rows, ch]) + dot_nt(
                qd[rows, ch], st_in[n, h])

    for s in range(steps):
        if s > 0:
            send_state(s)

        @pl.when(me >= 2 ** s)
        def _(s=s):
            for copy in state_copies(s):
                copy.wait_recv()
            for h in range(heads):
                ch = slice(h * KEY_FEATURE_DIM, (h + 1) * KEY_FEATURE_DIM)
                got = s_recv[s, h].astype(F32)
                exc_s[h] = got * exc_f[0:1, ch] + exc_s[h]
                inc_s[h] = got * inc_f[0:1, ch] + inc_s[h]
            exc_f[...] = exc_f[...] * f_recv[s]
            inc_f[...] = inc_f[...] * f_recv[s]

    for h in range(heads):
        ch = slice(h * KEY_FEATURE_DIM, (h + 1) * KEY_FEATURE_DIM)
        out = within[:, ch] + dot_nt(rw[:, ch], exc_s[h].astype(BF16))
        mean_sq = jnp.mean(out * out, axis=-1, keepdims=True)
        out = (out * lax.rsqrt(mean_sq + EPSILON) * gain_ref[:, ch]).astype(BF16)
        for t in range(n_tp):
            attn[t, :, ch] = out[t * row_count : (t + 1) * row_count]

    def attn_copy(i):
        to = lax.rem(tp + i, n_tp)
        return pltpu.make_async_remote_copy(
            attn.at[to], arecv.at[tp], as_sem.at[i], ar_sem.at[i],
            device_id=(me, to), device_id_type=MESH)

    for i in range(1, n_tp):
        attn_copy(i).start()
    arecv[tp] = attn[tp]
    for s in range(steps):
        @pl.when(me + 2 ** s < n_sp)
        def _(s=s):
            for copy in state_copies(s):
                copy.wait_send()
    ow_copy.wait()
    for i in range(1, n_tp):
        attn_copy(i).wait_recv()
    x = jnp.concatenate([arecv[t] for t in range(n_tp)], axis=1)
    tile = 512
    total = jnp.zeros((row_count, 1), F32)
    for c in range(0, model, tile):
        cs = slice(c, c + tile)
        mixed = (stream_ref[:, cs].astype(F32) + dot(x, ow[:, cs])).astype(BF16)
        mixed_ref[:, cs] = mixed
        mixed32 = mixed.astype(F32)
        total = total + jnp.sum(mixed32 * mixed32, axis=1, keepdims=True)
    inv = lax.rsqrt(total / model + EPSILON)
    for c in range(0, model, tile):
        cs = slice(c, c + tile)
        normed = (mixed_ref[:, cs].astype(F32) * inv * ffn_ref[:, cs]).astype(BF16)
        rows_ref[:, cs] = dot_tn(gsel, normed).astype(BF16)
    for i in range(1, n_tp):
        attn_copy(i).wait_send()


def experts_kernel(
    n_tp, per_group,
    rows_ref, wc_ref, gsel_ref, mixed_ref, gate_hbm, up_hbm, down_hbm,
    out_ref,
    gate, up, down, zrow, zw, stage, xbuf, hid, ybuf, back, ret, zret,
    w_sem, zs_sem, zr_sem, ws_sem, wr_sem, ps_sem, pr_sem, bs_sem, br_sem, rs_sem, rr_sem,
):
    idx = lax.axis_index("sp") * n_tp + lax.axis_index("tp")
    z, p = idx // per_group, lax.rem(idx, per_group)
    cap = zrow.shape[1]
    capp = stage.shape[2]
    slots = per_group * capp
    model = out_ref.shape[1]
    ff = hid.shape[1]

    def device(plane, place):
        flat = plane * per_group + place
        return (flat // n_tp, lax.rem(flat, n_tp))

    weights = [
        pltpu.make_async_copy(gate_hbm.at[0], gate, w_sem.at[0]),
        pltpu.make_async_copy(up_hbm.at[0], up, w_sem.at[1]),
        pltpu.make_async_copy(down_hbm.at[0], down, w_sem.at[2]),
    ]
    barrier = pltpu.get_barrier_semaphore()
    for i in range(1, GROUPS):
        pl.semaphore_signal(
            barrier, inc=1, device_id=device(lax.rem(z + i, GROUPS), p), device_id_type=MESH)

    @pl.loop(1, per_group)
    def _(i):
        pl.semaphore_signal(
            barrier, inc=1, device_id=device(z, lax.rem(p + i, per_group)), device_id_type=MESH)

    for copy in weights:
        copy.start()
    pl.semaphore_wait(barrier, GROUPS - 1 + per_group - 1)

    def plane_rows(k):
        to = lax.rem(z + k, GROUPS)
        return (
            pltpu.make_async_remote_copy(
                wc_ref.at[pl.ds(pl.multiple_of(to * cap, cap), cap)], zw.at[k],
                ws_sem.at[k], wr_sem.at[k], device_id=device(to, p), device_id_type=MESH),
            pltpu.make_async_remote_copy(
                rows_ref.at[pl.ds(pl.multiple_of(to * cap, cap), cap)], zrow.at[k],
                zs_sem.at[k], zr_sem.at[k], device_id=device(to, p), device_id_type=MESH),
        )

    def plane_return(k):
        to = lax.rem(z + GROUPS - k, GROUPS)
        return pltpu.make_async_remote_copy(
            ret.at[k], zret.at[k], rs_sem.at[k], rr_sem.at[k],
            device_id=device(to, p), device_id_type=MESH)

    def piece(k, i):
        to = lax.rem(p + i, per_group)
        return pltpu.make_async_remote_copy(
            stage.at[k, to], xbuf.at[k, p], ps_sem.at[k, i], pr_sem.at[k, i],
            device_id=device(z, to), device_id_type=MESH)

    def piece_back(k, i):
        to = lax.rem(p + i, per_group)
        return pltpu.make_async_remote_copy(
            ybuf.at[k, to], back.at[k, p], bs_sem.at[k, i], br_sem.at[k, i],
            device_id=device(z, to), device_id_type=MESH)

    for k in range(1, GROUPS):
        for copy in plane_rows(k):
            copy.start()
    own = pl.ds(pl.multiple_of(z * cap, cap), cap)
    zrow[0] = rows_ref[own, :]
    zw[0] = wc_ref[own, :]
    tile = 512

    def dispatch(k):
        if k > 0:
            for copy in plane_rows(k):
                copy.wait_recv()
        sel = (zw[k].astype(F32) > 0).astype(F32).astype(BF16)
        for c in range(0, model, tile):
            cs = slice(c, c + tile)
            stage[k, :, :, cs] = dot_tn(sel, zrow[k, :, cs]).astype(BF16).reshape(
                per_group, capp, tile)

        @pl.loop(1, per_group)
        def _(i):
            piece(k, i).start()

        xbuf[k, p] = stage[k, p]

    def expert(k):
        @pl.loop(1, per_group)
        def _(i):
            piece(k, i).wait_recv()

        x = xbuf.at[k]

        @pl.loop(0, ff // 256)
        def _(f):
            fs = pl.ds(pl.multiple_of(f * 256, 256), 256)
            rows = x[...].reshape(slots, model)
            g = dot(rows, gate[:, fs])
            u = dot(rows, up[:, fs])
            hid[:, fs] = (g / (1.0 + jnp.exp(-g)) * u).astype(BF16)

        @pl.loop(0, model // tile)
        def _(c):
            cs = pl.ds(pl.multiple_of(c * tile, tile), tile)
            ybuf[k, :, :, cs] = dot(hid[...], down[:, cs]).astype(BF16).reshape(
                per_group, capp, tile)

        @pl.loop(1, per_group)
        def _(i):
            piece_back(k, i).start()

        back[k, p] = ybuf[k, p]

    def combine(k):
        @pl.loop(1, per_group)
        def _(i):
            piece_back(k, i).wait_recv()

        w = zw[k]
        for c in range(0, model, tile):
            cs = slice(c, c + tile)
            y = dot(w, back[k, :, :, cs].reshape(slots, tile)).astype(BF16)
            if k == 0:
                zret[0, :, cs] = y
            else:
                ret[k, :, cs] = y
        if k > 0:
            plane_return(k).start()

    dispatch(0)
    for copy in weights:
        copy.wait()
    dispatch(1)
    expert(0)
    dispatch(2)
    expert(1)
    combine(0)
    dispatch(3)
    combine(1)
    expert(2)
    combine(2)
    expert(3)
    combine(3)

    for k in range(1, GROUPS):
        plane_return(k).wait_recv()
    gsel = [
        gsel_ref[:, g * cap : (g + 1) * cap] for g in range(GROUPS)
    ]
    for c in range(0, model, tile):
        cs = slice(c, c + tile)
        acc = mixed_ref[:, cs].astype(F32)
        for g in range(GROUPS):
            acc = acc + dot(gsel[g], zret[lax.rem(g - z + GROUPS, GROUPS), :, cs])
        out_ref[:, cs] = acc.astype(BF16)

    for k in range(1, GROUPS):
        for copy in plane_rows(k):
            copy.wait_send()
        plane_return(k).wait_send()
    for k in range(GROUPS):
        @pl.loop(1, per_group)
        def _(i, k=k):
            piece(k, i).wait_send()
            piece_back(k, i).wait_send()


def local(
    stream, query_rows, key_rows, value_rows, log_decay, head_gain, out_weight, ffn_gain,
    expert_ids, group_prob, pick_logits, gate_weight, up_weight, down_weight,
):
    n_sp, n_tp = lax.axis_size("sp"), lax.axis_size("tp")
    tokens, cols = query_rows.shape
    heads = cols // KEY_FEATURE_DIM
    blocks = tokens // BLOCK
    row_count, model = stream.shape
    devices = n_sp * n_tp
    per_group = devices // GROUPS
    cap = 2 * row_count * TOPK // devices
    capp = -(-cap // 16) * 16
    group_cap = per_group * cap // TOPK
    slots = per_group * capp
    ff = gate_weight.shape[2]
    steps = max(1, (n_sp - 1).bit_length())
    kd = KEY_FEATURE_DIM
    vm = pl.BlockSpec(memory_space=pltpu.VMEM)
    anyspace = pl.BlockSpec(memory_space=pl.ANY)
    dma = pltpu.SemaphoreType.DMA
    mixed, rows, wc, gsel = pl.pallas_call(
        functools.partial(mixer_kernel, n_sp, n_tp, capp),
        out_shape=(
            jax.ShapeDtypeStruct((row_count, model), BF16),
            jax.ShapeDtypeStruct((GROUPS * group_cap, model), BF16),
            jax.ShapeDtypeStruct((GROUPS * group_cap, slots), BF16),
            jax.ShapeDtypeStruct((row_count, GROUPS * group_cap), BF16),
        ),
        in_specs=[vm] * 6 + [anyspace] + [vm] * 4,
        out_specs=(vm,) * 4,
        scratch_shapes=[
            pltpu.VMEM((tokens, cols), BF16),
            pltpu.VMEM((tokens, cols), BF16),
            pltpu.VMEM((tokens, cols), BF16),
            pltpu.VMEM((blocks, heads, kd, kd), BF16),
            pltpu.VMEM((tokens, cols), F32),
            pltpu.VMEM(out_weight.shape, BF16),
            pltpu.VMEM((heads, kd, kd), F32),
            pltpu.VMEM((8, cols), F32),
            pltpu.VMEM((heads, kd, kd), F32),
            pltpu.VMEM((8, cols), F32),
            pltpu.VMEM((steps, heads, kd, kd), BF16),
            pltpu.VMEM((steps, heads, kd, kd), BF16),
            pltpu.VMEM((steps, 8, cols), F32),
            pltpu.VMEM((steps, 8, cols), F32),
            pltpu.VMEM((n_tp, row_count, cols), BF16),
            pltpu.VMEM((n_tp, row_count, cols), BF16),
            dma,
            dma((steps,)), dma((steps,)), dma((steps,)), dma((steps,)),
            dma((n_tp,)), dma((n_tp,)),
        ],
        compiler_params=pltpu.CompilerParams(
            collective_id=0, has_side_effects=True, vmem_limit_bytes=VMEM_LIMIT),
    )(
        query_rows, key_rows, value_rows, log_decay, head_gain[None], stream, out_weight,
        ffn_gain[None], expert_ids, group_prob[:, None], pick_logits,
    )
    return pl.pallas_call(
        functools.partial(experts_kernel, n_tp, per_group),
        out_shape=jax.ShapeDtypeStruct((row_count, model), BF16),
        in_specs=[vm] * 4 + [anyspace] * 3,
        out_specs=vm,
        scratch_shapes=[
            pltpu.VMEM((model, ff), BF16),
            pltpu.VMEM((model, ff), BF16),
            pltpu.VMEM((ff, model), BF16),
            pltpu.VMEM((GROUPS, group_cap, model), BF16),
            pltpu.VMEM((GROUPS, group_cap, slots), BF16),
            pltpu.VMEM((GROUPS, per_group, capp, model), BF16),
            pltpu.VMEM((GROUPS, per_group, capp, model), BF16),
            pltpu.VMEM((slots, ff), BF16),
            pltpu.VMEM((GROUPS, per_group, capp, model), BF16),
            pltpu.VMEM((GROUPS, per_group, capp, model), BF16),
            pltpu.VMEM((GROUPS, group_cap, model), BF16),
            pltpu.VMEM((GROUPS, group_cap, model), BF16),
            dma((3,)),
            dma((GROUPS,)), dma((GROUPS,)), dma((GROUPS,)), dma((GROUPS,)),
            dma((GROUPS, per_group)), dma((GROUPS, per_group)),
            dma((GROUPS, per_group)), dma((GROUPS, per_group)),
            dma((GROUPS,)), dma((GROUPS,)),
        ],
        compiler_params=pltpu.CompilerParams(
            collective_id=1, has_side_effects=True, vmem_limit_bytes=VMEM_LIMIT),
    )(rows, wc, gsel, mixed, gate_weight, up_weight, down_weight)


def solution(mesh):
    in_specs = (
        P(("sp", "tp"), None),
        P("sp", "tp"),
        P("sp", "tp"),
        P("sp", "tp"),
        P("sp", "tp"),
        P("tp"),
        P(),
        P(),
        P(("sp", "tp"), None),
        P(("sp", "tp")),
        P(("sp", "tp"), None),
        P(("sp", "tp"), None, None),
        P(("sp", "tp"), None, None),
        P(("sp", "tp"), None, None),
    )
    out_specs = P(("sp", "tp"), None)
    return jax.shard_map(local, mesh=mesh, in_specs=in_specs, out_specs=out_specs, check_vma=False)
```

time: 224 us -> 107 us (0.48)
  Pallas kernels: 0 us -> 101 us
  blocking collectives: 74.2 us -> 0 us
  waiting for transfers between devices: 70.8 us -> 0 us
  matrix products: 21 us -> 0 us
  other arithmetic: 20 us -> 0 us
  between operations: 13.8 us -> 0.02 us
  local copies, waits for them, and re-layouts: 16.2 us -> 6.08 us
  starting transfers between devices: 7.18 us -> 0 us
    pallas_call x0 -> x2, Pallas kernels: none -> 101 us  [the longest x1 84.4 us: local(): pl.pallas_call(functools.partial(experts_kernel, n_tp, per_group), out_sh...]
    all_to_all x2 -> x0, waiting for transfers between devices: 54.4 us -> none  [the longest x1 48.7 us: local(): lax.all_to_all(served, ('sp', 'tp'), split_axis=0, concat_axis=0, tiled=T...]
    all_to_all x1 -> x0, blocking collectives: 51.9 us -> none  [local(): lax.all_to_all(outgoing.reshape(devices, EXP_DEV, slot_cap, model_width),...]
    all_gather x1 -> x0, blocking collectives: 22.3 us -> none  [entering_2(): everything = jax.tree.map(lambda part: lax.all_gather(part, axis), value)]
    dot_general x8 -> x0, matrix products: 21 us -> none  [the longest x1 10 us: run_experts(): jnp.einsum('sekf,efd->sekd', hidden, down_weight, preferred_element_type=...]
    all_gather x1 -> x0, waiting for transfers between devices: 16.3 us -> none  [entering_2(): everything = jax.tree.map(lambda part: lax.all_gather(part, axis), value)]
    select_n x11 -> x0, other arithmetic: 8.3 us -> none  [the longest x8 8.28 us: turn(): return jax.tree.map(lambda a, b: jnp.where(reached, a, b), new, before)]
    all_to_all x2 -> x0, starting transfers between devices: 7.17 us -> none  [the longest x1 3.59 us: local(): lax.all_to_all(attn_rows.reshape(tp_size, row_count, head_cols), 'tp', sp...]
  transfers between devices with their start and end apart: 3 -> 0, of which waited for: 3 -> 0; matrix products, arithmetic and copies ran while one was open for 2% -> 0% of each run, Pallas kernels for 0% -> 0%
where the time goes in v1:
time: 107 us
  Pallas kernels  101 us (94%)
  local copies, waits for them, and re-layouts  6.08 us (6%)
    pallas_call x1, Pallas kernels, local(): pl.pallas_call(functools.partial(experts_kernel, n_tp, per_group), out_sh...  84.4 us
    pallas_call x1, Pallas kernels, local(): pl.pallas_call(functools.partial(mixer_kernel, n_sp, n_tp, capp), out_sha...  16.3 us
    unnamed x3, local copies, waits for them, and re-layouts  4.69 us

profile of v1, /device:TPU:0, one launch (start us, length us, event | category | flops | bytes accessed | tf_op | source)
XLA Modules:
  0.0 106.8 jit_solution(18193912331892180095)
XLA Ops:
  0.0 1.4 %copy.15.ids_ref = s32[128,2]{1,0:T(8,128)} copy(s32[128,2]{0,1:T(2,128)} %param.22) | data formatting | bytes 2048 | tf_op args[8]
  1.4 1.4 %copy.16.prob_ref = f32[128,1]{1,0:T(8,128)} copy(f32[128,1]{0,1:T(1,128)} %bitcast.5) | data formatting | bytes 1024 | tf_op jit(solution)/shard_map/broadcast_in_dim | solution.py:443
  2.8 1.4 %copy.17.logit_ref = f32[128,2]{1,0:T(8,128)} copy(f32[128,2]{0,1:T(2,128)} %param.24) | data formatting | bytes 2048 | tf_op args[10]
  4.2 16.3 %shard_map.136 = (bf16[128,2048]{1,0:T(8,128)(2,1)}, bf16[256,2048]{1,0:T(8,128)(2,1)}, bf16[256,128]{1,0:T(8,128)(2,1)}, bf16[128,256]{1,0:T(8,128)(2,1)}) custom-call(bf16[512,256]{1,0:T(8,128)(2,1)} %q_ref.1, bf16[512,256]{1,0:T(8,128)(2,1)} %k_ref.1, bf16[512,256]{1,0:T(8,128)(2,1)} %v_ref.1, f32[512,256]{1,0:T(8,128)} %decay_ref.1, f32[1,256]{1,0:T(1,128)} %bitcast.4, ...), custom_call_target="tpu_custom_call" | custom-call | tf_op jit(solution)/shard_map/pallas_call | solution.py:408
  20.5 84.4 %shard_map.137 = bf16[128,2048]{1,0:T(8,128)(2,1)} custom-call(bf16[256,2048]{1,0:T(8,128)(2,1)} %get-tuple-element.9.rows_ref, bf16[256,128]{1,0:T(8,128)(2,1)} %get-tuple-element.10.wc_ref, bf16[128,256]{1,0:T(8,128)(2,1)} %get-tuple-element.11.gsel_ref, bf16[128,2048]{1,0:T(8,128)(2,1)} %get-tuple-element.12.mixed_ref, bf16[1,2048,1024]{2,1,0:T(8,128)(2,1)} %gate_hbm.1, ...), custom_call_target="tpu_custom_call" | custom-call | tf_op jit(solution)/shard_map/pallas_call | solution.py:445
  104.9 1.9 %copy.19 = bf16[128,2048]{1,0:T(8,128)(2,1)} copy(bf16[128,2048]{1,0:T(8,128)(2,1)} %shard_map.137) | data formatting | bytes 1048576

commit v2 on v1

--- a/solution.py
+++ b/solution.py
@@ -15,7 +15,8 @@
 F32 = jnp.float32
 BF16 = jnp.bfloat16
 MESH = pl.DeviceIdType.MESH
-VMEM_LIMIT = 60 * 1024 * 1024
+VMEM_LIMIT = 63 * 1024 * 1024
+SCHEDULE = "D0 W D1 E0 D2 E1 C0 D3 C1 E2 C2 E3 C3"
 
 
 def dot(a, b):
@@ -34,11 +35,11 @@
     return lax.broadcasted_iota(jnp.int32, shape, axis)
 
 
-def mixer_kernel(
-    n_sp, n_tp, capp,
+def mixer_part(
+    n_sp, n_tp, capp, greet,
     q_ref, k_ref, v_ref, decay_ref, gain_ref, stream_ref, ow_hbm, ffn_ref, ids_ref, prob_ref,
     logit_ref,
-    mixed_ref, rows_ref, wc_ref, gsel_ref,
+    mixed_ref, rows_ref, wc_ref, gsel_ref, weights,
     qd, kd, rw, st_in, within, ow, inc_s, inc_f, exc_s, exc_f,
     s_send, s_recv, f_send, f_recv, attn, arecv,
     ow_sem, ss_sem, sr_sem, fs_sem, fr_sem, as_sem, ar_sem,
@@ -58,8 +59,11 @@
     for i in range(1, n_tp):
         pl.semaphore_signal(
             barrier, inc=1, device_id=(me, lax.rem(tp + i, n_tp)), device_id_type=MESH)
+    greet()
     ow_copy = pltpu.make_async_copy(ow_hbm, ow, ow_sem)
     ow_copy.start()
+    for copy in weights:
+        copy.start()
 
     tri = (iota((BLOCK, BLOCK), 0) >= iota((BLOCK, BLOCK), 1)).astype(F32)
     tri16 = tri.astype(BF16)
@@ -93,7 +97,7 @@
     inc_f[...] = jnp.broadcast_to(jnp.exp(start), inc_f.shape)
     exc_f[...] = jnp.ones_like(exc_f)
 
-    pl.semaphore_wait(barrier, n_sp - 1 + n_tp - 1)
+    pl.semaphore_wait(barrier, n_sp - 1 + n_tp - 1 + GROUPS - 1 + n_sp * n_tp // GROUPS - 1)
 
     def state_copies(s):
         to = (lax.rem(me + 2 ** s, n_sp), tp)
@@ -121,29 +125,27 @@
     per_group = experts // GROUPS
     group_cap = rows_ref.shape[0] // GROUPS
     slots = per_group * capp
-    ids = ids_ref[...]
-    id0, id1 = ids[:, 0:1], ids[:, 1:2]
-    oh0 = (iota((row_count, experts), 1) == id0).astype(F32)
-    oh1 = (iota((row_count, experts), 1) == id1).astype(F32)
-    before = (iota((row_count, row_count), 0) > iota((row_count, row_count), 1)).astype(BF16)
-    counts = dot(before, (oh0 + oh1).astype(BF16))
-    rank0 = jnp.sum(counts * oh0, axis=1, keepdims=True).astype(jnp.int32)
-    rank1 = jnp.sum(counts * oh1, axis=1, keepdims=True).astype(jnp.int32)
+    id0, id1 = ids_ref[0:1, :], ids_ref[1:2, :]
+    oh0 = (iota((experts, row_count), 0) == id0).astype(F32)
+    oh1 = (iota((experts, row_count), 0) == id1).astype(F32)
+    before = (iota((row_count, row_count), 0) < iota((row_count, row_count), 1)).astype(BF16)
+    counts = dot((oh0 + oh1).astype(BF16), before)
+    rank0 = jnp.sum(counts * oh0, axis=0, keepdims=True).astype(jnp.int32)
+    rank1 = jnp.sum(counts * oh1, axis=0, keepdims=True).astype(jnp.int32)
     group = id0 // per_group
-    ohg = (iota((row_count, KEY_FEATURE_DIM), 1) == group).astype(F32)
-    rank_g = jnp.sum(dot(before, ohg.astype(BF16)) * ohg, axis=1, keepdims=True).astype(jnp.int32)
+    ohg = (iota((16, row_count), 0) == group).astype(F32)
+    rank_g = jnp.sum(dot(ohg.astype(BF16), before) * ohg, axis=0, keepdims=True).astype(jnp.int32)
     place = group * group_cap + rank_g
-    gsel = (iota((row_count, GROUPS * group_cap), 1) == place).astype(F32).astype(BF16)
+    gsel = (iota((GROUPS * group_cap, row_count), 0) == place).astype(F32).astype(BF16)
     gsel_ref[...] = gsel
     slot0 = (id0 - group * per_group) * capp + rank0
     slot1 = (id1 - group * per_group) * capp + rank1
-    logits = logit_ref[...]
-    gap = logits[:, 0:1] - logits[:, 1:2]
+    gap = logit_ref[0:1, :] - logit_ref[1:2, :]
     w0 = prob_ref[...] / (1.0 + jnp.exp(-gap))
     w1 = prob_ref[...] / (1.0 + jnp.exp(gap))
-    slot_iota = iota((row_count, slots), 1)
+    slot_iota = iota((slots, row_count), 0)
     w_tok = jnp.where(slot_iota == slot0, w0, 0.0) + jnp.where(slot_iota == slot1, w1, 0.0)
-    wc_ref[...] = dot_tn(gsel, w_tok.astype(BF16)).astype(BF16)
+    wc_ref[...] = dot_nt(gsel, w_tok.astype(BF16)).astype(BF16)
 
     for n in range(blocks):
         rows = slice(n * BLOCK, (n + 1) * BLOCK)
@@ -207,22 +209,24 @@
     for c in range(0, model, tile):
         cs = slice(c, c + tile)
         normed = (mixed_ref[:, cs].astype(F32) * inv * ffn_ref[:, cs]).astype(BF16)
-        rows_ref[:, cs] = dot_tn(gsel, normed).astype(BF16)
+        rows_ref[:, cs] = dot(gsel_ref[...], normed).astype(BF16)
     for i in range(1, n_tp):
         attn_copy(i).wait_send()
 
 
-def experts_kernel(
-    n_tp, per_group,
-    rows_ref, wc_ref, gsel_ref, mixed_ref, gate_hbm, up_hbm, down_hbm,
+def layer_kernel(
+    n_sp, n_tp, per_group, capp,
+    q_ref, k_ref, v_ref, decay_ref, gain_ref, stream_ref, ow_hbm, ffn_ref, ids_ref, prob_ref,
+    logit_ref, gate_hbm, up_hbm, down_hbm,
     out_ref,
+    mixed_ref, rows_ref, wc_ref, gsel_ref,
     gate, up, down, zrow, zw, stage, xbuf, hid, ybuf, back, ret, zret,
     w_sem, zs_sem, zr_sem, ws_sem, wr_sem, ps_sem, pr_sem, bs_sem, br_sem, rs_sem, rr_sem,
+    *mixer_scratch,
 ):
     idx = lax.axis_index("sp") * n_tp + lax.axis_index("tp")
     z, p = idx // per_group, lax.rem(idx, per_group)
     cap = zrow.shape[1]
-    capp = stage.shape[2]
     slots = per_group * capp
     model = out_ref.shape[1]
     ff = hid.shape[1]
@@ -236,19 +240,22 @@
         pltpu.make_async_copy(up_hbm.at[0], up, w_sem.at[1]),
         pltpu.make_async_copy(down_hbm.at[0], down, w_sem.at[2]),
     ]
-    barrier = pltpu.get_barrier_semaphore()
-    for i in range(1, GROUPS):
-        pl.semaphore_signal(
-            barrier, inc=1, device_id=device(lax.rem(z + i, GROUPS), p), device_id_type=MESH)
-
-    @pl.loop(1, per_group)
-    def _(i):
-        pl.semaphore_signal(
-            barrier, inc=1, device_id=device(z, lax.rem(p + i, per_group)), device_id_type=MESH)
-
-    for copy in weights:
-        copy.start()
-    pl.semaphore_wait(barrier, GROUPS - 1 + per_group - 1)
+    def greet():
+        barrier = pltpu.get_barrier_semaphore()
+        for i in range(1, GROUPS):
+            pl.semaphore_signal(
+                barrier, inc=1, device_id=device(lax.rem(z + i, GROUPS), p), device_id_type=MESH)
+
+        @pl.loop(1, per_group)
+        def _(i):
+            pl.semaphore_signal(
+                barrier, inc=1, device_id=device(z, lax.rem(p + i, per_group)),
+                device_id_type=MESH)
+
+    mixer_part(
+        n_sp, n_tp, capp, greet,
+        q_ref, k_ref, v_ref, decay_ref, gain_ref, stream_ref, ow_hbm, ffn_ref, ids_ref, prob_ref,
+        logit_ref, mixed_ref, rows_ref, wc_ref, gsel_ref, weights, *mixer_scratch)
 
     def plane_rows(k):
         to = lax.rem(z + k, GROUPS)
@@ -264,7 +271,7 @@
     def plane_return(k):
         to = lax.rem(z + GROUPS - k, GROUPS)
         return pltpu.make_async_remote_copy(
-            ret.at[k], zret.at[k], rs_sem.at[k], rr_sem.at[k],
+            ret.at[k], zret.at[z], rs_sem.at[k], rr_sem.at[k],
             device_id=device(to, p), device_id_type=MESH)
 
     def piece(k, i):
@@ -340,38 +347,25 @@
             cs = slice(c, c + tile)
             y = dot(w, back[k, :, :, cs].reshape(slots, tile)).astype(BF16)
             if k == 0:
-                zret[0, :, cs] = y
+                zret[z, :, cs] = y
             else:
                 ret[k, :, cs] = y
         if k > 0:
             plane_return(k).start()
 
-    dispatch(0)
-    for copy in weights:
-        copy.wait()
-    dispatch(1)
-    expert(0)
-    dispatch(2)
-    expert(1)
-    combine(0)
-    dispatch(3)
-    combine(1)
-    expert(2)
-    combine(2)
-    expert(3)
-    combine(3)
+    for step in SCHEDULE.split():
+        if step == "W":
+            for copy in weights:
+                copy.wait()
+        else:
+            {"D": dispatch, "E": expert, "C": combine}[step[0]](int(step[1]))
 
     for k in range(1, GROUPS):
         plane_return(k).wait_recv()
-    gsel = [
-        gsel_ref[:, g * cap : (g + 1) * cap] for g in range(GROUPS)
-    ]
     for c in range(0, model, tile):
         cs = slice(c, c + tile)
-        acc = mixed_ref[:, cs].astype(F32)
-        for g in range(GROUPS):
-            acc = acc + dot(gsel[g], zret[lax.rem(g - z + GROUPS, GROUPS), :, cs])
-        out_ref[:, cs] = acc.astype(BF16)
+        moved = dot_tn(gsel_ref[...], zret[:, :, cs].reshape(GROUPS * cap, tile))
+        out_ref[:, cs] = (mixed_ref[:, cs].astype(F32) + moved).astype(BF16)
 
     for k in range(1, GROUPS):
         for copy in plane_rows(k):
@@ -405,49 +399,37 @@
     vm = pl.BlockSpec(memory_space=pltpu.VMEM)
     anyspace = pl.BlockSpec(memory_space=pl.ANY)
     dma = pltpu.SemaphoreType.DMA
-    mixed, rows, wc, gsel = pl.pallas_call(
-        functools.partial(mixer_kernel, n_sp, n_tp, capp),
-        out_shape=(
-            jax.ShapeDtypeStruct((row_count, model), BF16),
-            jax.ShapeDtypeStruct((GROUPS * group_cap, model), BF16),
-            jax.ShapeDtypeStruct((GROUPS * group_cap, slots), BF16),
-            jax.ShapeDtypeStruct((row_count, GROUPS * group_cap), BF16),
-        ),
-        in_specs=[vm] * 6 + [anyspace] + [vm] * 4,
-        out_specs=(vm,) * 4,
-        scratch_shapes=[
-            pltpu.VMEM((tokens, cols), BF16),
-            pltpu.VMEM((tokens, cols), BF16),
-            pltpu.VMEM((tokens, cols), BF16),
-            pltpu.VMEM((blocks, heads, kd, kd), BF16),
-            pltpu.VMEM((tokens, cols), F32),
-            pltpu.VMEM(out_weight.shape, BF16),
-            pltpu.VMEM((heads, kd, kd), F32),
-            pltpu.VMEM((8, cols), F32),
-            pltpu.VMEM((heads, kd, kd), F32),
-            pltpu.VMEM((8, cols), F32),
-            pltpu.VMEM((steps, heads, kd, kd), BF16),
-            pltpu.VMEM((steps, heads, kd, kd), BF16),
-            pltpu.VMEM((steps, 8, cols), F32),
-            pltpu.VMEM((steps, 8, cols), F32),
-            pltpu.VMEM((n_tp, row_count, cols), BF16),
-            pltpu.VMEM((n_tp, row_count, cols), BF16),
-            dma,
-            dma((steps,)), dma((steps,)), dma((steps,)), dma((steps,)),
-            dma((n_tp,)), dma((n_tp,)),
-        ],
-        compiler_params=pltpu.CompilerParams(
-            collective_id=0, has_side_effects=True, vmem_limit_bytes=VMEM_LIMIT),
-    )(
-        query_rows, key_rows, value_rows, log_decay, head_gain[None], stream, out_weight,
-        ffn_gain[None], expert_ids, group_prob[:, None], pick_logits,
-    )
+    mixer_scratch = [
+        pltpu.VMEM((tokens, cols), BF16),
+        pltpu.VMEM((tokens, cols), BF16),
+        pltpu.VMEM((tokens, cols), BF16),
+        pltpu.VMEM((blocks, heads, kd, kd), BF16),
+        pltpu.VMEM((tokens, cols), F32),
+        pltpu.VMEM(out_weight.shape, BF16),
+        pltpu.VMEM((heads, kd, kd), F32),
+        pltpu.VMEM((8, cols), F32),
+        pltpu.VMEM((heads, kd, kd), F32),
+        pltpu.VMEM((8, cols), F32),
+        pltpu.VMEM((steps, heads, kd, kd), BF16),
+        pltpu.VMEM((steps, heads, kd, kd), BF16),
+        pltpu.VMEM((steps, 8, cols), F32),
+        pltpu.VMEM((steps, 8, cols), F32),
+        pltpu.VMEM((n_tp, row_count, cols), BF16),
+        pltpu.VMEM((n_tp, row_count, cols), BF16),
+        dma,
+        dma((steps,)), dma((steps,)), dma((steps,)), dma((steps,)),
+        dma((n_tp,)), dma((n_tp,)),
+    ]
     return pl.pallas_call(
-        functools.partial(experts_kernel, n_tp, per_group),
+        functools.partial(layer_kernel, n_sp, n_tp, per_group, capp),
         out_shape=jax.ShapeDtypeStruct((row_count, model), BF16),
-        in_specs=[vm] * 4 + [anyspace] * 3,
+        in_specs=[vm] * 6 + [anyspace] + [vm] * 4 + [anyspace] * 3,
         out_specs=vm,
         scratch_shapes=[
+            pltpu.VMEM((row_count, model), BF16),
+            pltpu.VMEM((GROUPS * group_cap, model), BF16),
+            pltpu.VMEM((GROUPS * group_cap, slots), BF16),
+            pltpu.VMEM((GROUPS * group_cap, row_count), BF16),
             pltpu.VMEM((model, ff), BF16),
             pltpu.VMEM((model, ff), BF16),
             pltpu.VMEM((ff, model), BF16),
@@ -465,10 +447,14 @@
             dma((GROUPS, per_group)), dma((GROUPS, per_group)),
             dma((GROUPS, per_group)), dma((GROUPS, per_group)),
             dma((GROUPS,)), dma((GROUPS,)),
-        ],
+        ] + mixer_scratch,
         compiler_params=pltpu.CompilerParams(
-            collective_id=1, has_side_effects=True, vmem_limit_bytes=VMEM_LIMIT),
-    )(rows, wc, gsel, mixed, gate_weight, up_weight, down_weight)
+            collective_id=0, has_side_effects=True, vmem_limit_bytes=VMEM_LIMIT),
+    )(
+        query_rows, key_rows, value_rows, log_decay, head_gain[None], stream, out_weight,
+        ffn_gain[None], expert_ids.T, group_prob[None], pick_logits.T,
+        gate_weight, up_weight, down_weight,
+    )
 
 
 def solution(mesh):

time: 107 us -> 97.2 us (0.908)
  Pallas kernels: 101 us -> 94.2 us
  local copies, waits for them, and re-layouts: 6.08 us -> 1.88 us
    pallas_call x2 -> x1, Pallas kernels: 101 us -> 94.2 us  [local(): pl.pallas_call(functools.partial(layer_kernel, n_sp, n_tp, per_group, cap...]
    unnamed x3 -> x1, local copies, waits for them, and re-layouts: 4.69 us -> 1.88 us
    broadcast_in_dim x1 -> x0, local copies, waits for them, and re-layouts: 1.38 us -> none  [local(): group_prob[:, None]]
where the time goes in v2:
time: 97.2 us; the launch traced here: 96.1 us
  Pallas kernels  94.2 us (97%)
  local copies, waits for them, and re-layouts  1.88 us (2%)
    pallas_call x1, Pallas kernels, local(): pl.pallas_call(functools.partial(layer_kernel, n_sp, n_tp, per_group, cap...  94.2 us

profile of v2, /device:TPU:0, one launch (start us, length us, event | category | flops | bytes accessed | tf_op | source)
XLA Modules:
  0.0 96.1 jit_solution(17227360063299216177)
XLA Ops:
  0.0 94.2 %shard_map.136 = bf16[128,2048]{1,0:T(8,128)(2,1)} custom-call(bf16[512,256]{1,0:T(8,128)(2,1)} %q_ref.1, bf16[512,256]{1,0:T(8,128)(2,1)} %k_ref.1, bf16[512,256]{1,0:T(8,128)(2,1)} %v_ref.1, f32[512,256]{1,0:T(8,128)} %decay_ref.1, f32[1,256]{1,0:T(1,128)} %bitcast.6, bf16[128,2048]{1,0:T(8,128)(2,1)} %stream_ref.1, bf16[1024,2048]{1,0:T(8,128)(2,1)} %ow_hbm.1, ...), custom_call_target="tpu_custom_call" | custom-call | tf_op jit(solution)/shard_map/pallas_call | solution.py:423
  94.2 1.9 %copy.16 = bf16[128,2048]{1,0:T(8,128)(2,1)} copy(bf16[128,2048]{1,0:T(8,128)(2,1)} %shard_map.136) | data formatting | bytes 1048576
